TPU v7x, 128 devices: a whole 4x4x4 slice. The times are simulated.
128 devices in a mesh: rep: 2 (over z_hi), fs: 32 (over z_lo, y, x), tp: 2 (over core).
Axes of the slice: x: 4, y: 4, z: 4 (z_hi: 2, z_lo: 2; z = z_hi * 2 + z_lo), core: 2. Of those that a mesh axis runs over, the one named last changes fastest.
Arguments:
- tokens: bfloat16 [49152, 2048], P(('rep', 'fs', 'tp')), may hold values from -6 to 6
- outer_weight: float32 [2048, 1536], P('fs', 'tp'), may hold values from -0.125 to 0.125
- inner_weight: float32 [2048, 1536], P('fs', 'tp'), may hold values from -0.125 to 0.125
- value_weight: float32 [2048, 1536], P('fs', 'tp'), may hold values from -0.125 to 0.125
- conv_taps: float32 [3, 1536], P(None, 'tp'), may hold values from -3 to 3
- mix_out: float32 [1536, 2048], P('tp', 'fs'), may hold values from -0.15625 to 0.15625
- norm_first: float32 [2048], replicated, may hold values from 0.1 to 1.9
- up_weight: float32 [2048, 4096], P('fs', 'tp'), may hold values from -0.125 to 0.125
- down_weight: float32 [4096, 2048], P('tp', 'fs'), may hold values from -0.09375 to 0.09375
- norm_second: float32 [2048], replicated, may hold values from 0.1 to 1.9
Outputs:
- encoded: bfloat16 [49152, 2048], P(('rep', 'fs', 'tp'))
All inputs are finite; a program needn't handle non-finite values.
Results may differ from a plain program's by a relative error of at most 0.015.
Values may be sent and summed in bfloat16 or wider, within the bound.
No kernel may reach another device: no remote copies, remote signals or barrier semaphores. Data moves between devices by JAX's collectives and lax.ppermute only.
A program may use at most 128 MiB of HBM per device.

v0:
```python
import jax
import jax.numpy as jnp
from jax import lax
from jax.sharding import Mesh
from jax.sharding import PartitionSpec as P

SEQ = 128
FS = ("fs_0", "fs_1", "fs_2")
REP_FS = ("rep", "fs_0", "fs_1", "fs_2")
REP_FS_TP = ("rep", "fs_0", "fs_1", "fs_2", "tp")
residual_scale = 2.0**0.25
norm_epsilon = 1e-05


def own_half(x, dim):
    length = x.shape[dim] // 2
    return lax.dynamic_slice_in_dim(x, lax.axis_index("rep") * length, length, dim)


def gathered_halves(x):
    full = lax.all_gather(x, REP_FS, axis=0, tiled=True)
    return full.reshape(2, -1, x.shape[1])


def sum_at_owner(x, axis):
    tiles = x.reshape(2, -1, x.shape[1])
    arrived = lax.all_to_all(tiles, axis, split_axis=0, concat_axis=0, tiled=True)
    return arrived.astype(jnp.float32).sum(axis=0)


def layer_norm(values, scaling):
    center = values - jnp.mean(values, axis=-1, keepdims=True)
    spread = jnp.mean(center * center, axis=-1, keepdims=True)
    return center * lax.rsqrt(spread + norm_epsilon) * scaling


def short_conv(product, conv_taps):
    places = jnp.arange(product.shape[0], dtype=jnp.int32) % SEQ
    blank = jnp.zeros((1, product.shape[1]), jnp.float32)
    before = jnp.concatenate([blank, product[:-1]], axis=0)
    after = jnp.concatenate([product[1:], blank], axis=0)
    before = jnp.where((places > 0)[:, None], before, 0.0)
    after = jnp.where((places < SEQ - 1)[:, None], after, 0.0)
    return conv_taps[0] * before + conv_taps[1] * product + conv_taps[2] * after


def dot(a, b):
    return jnp.dot(a, b, preferred_element_type=jnp.float32)


def dot_t(a, b):
    return lax.dot_general(a, b, (((1,), (1,)), ((), ())), preferred_element_type=jnp.float32)


def local(
    tokens,
    outer_weight,
    inner_weight,
    value_weight,
    conv_taps,
    mix_out,
    norm_first,
    up_weight,
    down_weight,
    norm_second,
):
    bf = jnp.bfloat16
    grouped = lax.all_gather(tokens, "tp", axis=0, tiled=True)
    into = jnp.concatenate(
        [own_half(w, 1).astype(bf) for w in (outer_weight, inner_weight, value_weight)], axis=1
    )
    into_full = gathered_halves(into)
    mixout_full = gathered_halves(own_half(mix_out, 0).astype(bf).T)
    up_full = gathered_halves(own_half(up_weight, 1).astype(bf))
    down_full = gathered_halves(own_half(down_weight, 0).astype(bf).T)
    width = into.shape[1] // 3
    mixing = 0.0
    for h in range(2):
        w = into_full[h]
        outer = dot(grouped, w[:, :width])
        inner = dot(grouped, w[:, width : 2 * width])
        value = dot(grouped, w[:, 2 * width :])
        taps = conv_taps[:, h * width : (h + 1) * width]
        mixed = (outer * short_conv(inner * value, taps)).astype(bf)
        mixing = mixing + dot_t(mixed, mixout_full[h])
    mixing = sum_at_owner(mixing.astype(bf), "tp")
    first = layer_norm(residual_scale * tokens.astype(jnp.float32) + mixing, norm_first).astype(bf)
    grouped_first = lax.all_gather(first, "tp", axis=0, tiled=True)
    lowered = 0.0
    for h in range(2):
        raised = jax.nn.relu(dot(grouped_first, up_full[h]))
        hidden = (raised * raised).astype(bf)
        lowered = lowered + dot_t(hidden, down_full[h])
    lowered = sum_at_owner(lowered.astype(bf), "tp")
    return layer_norm(residual_scale * first.astype(jnp.float32) + lowered, norm_second).astype(bf)


def solution(mesh):
    finer = Mesh(
        mesh.devices.reshape(mesh.shape["rep"], 2, 4, 4, mesh.shape["tp"]),
        ("rep", "fs_0", "fs_1", "fs_2", "tp"),
    )
    placed = (
        P(REP_FS_TP, None),
        P(FS, "tp"),
        P(FS, "tp"),
        P(FS, "tp"),
        P(None, "tp"),
        P("tp", FS),
        P(),
        P(FS, "tp"),
        P("tp", FS),
        P(),
    )
    return jax.shard_map(
        local, mesh=finer, in_specs=placed, out_specs=P(REP_FS_TP, None), check_vma=False
    )
```

profile of v0, /device:TPU:1, one launch (start us, length us, event | category | flops | bytes accessed | tf_op | source)
XLA Modules:
  0.0 385.9 jit_solution(15496005332504647773)
XLA Ops:
  6.5 0.7 all-gather.9.cloned.1.call-update
  7.3 0.0 all-gather.7.cloned.1.call-start
  7.3 0.9 dynamic-slice_convert_fusion.5
  8.2 1.0 dynamic-slice_convert_fusion.3
  9.2 0.7 pad_maximum_fusion
  9.8 0.0 all-gather.7.cloned.1.call-update
  9.9 0.0 all-gather.11.cloned.1.call-start
  9.9 1.5 fusion.87
  11.4 0.0 all-gather.11.cloned.1.call-update
  11.5 0.0 all-gather.15.cloned.1.call-start
  11.5 0.7 dynamic-slice_convert_fusion.1
  12.2 0.0 all-gather.15.cloned.1.call-update
  12.2 0.0 all-gather.13.cloned.1.call-start
  12.3 0.8 slice_reduce_fusion.2
  13.1 14.3 %all-gather.9.cloned.1.call-done = bf16[768,2048]{1,0:T(8,128)(2,1)} async-done(((bf16[384,2048]{1,0:T(8,128)(2,1)}), bf16[768,2048]{1,0:T(8,128)(2,1)}) %all-gather.9.cloned.1.call-update) | async-done | bytes 3145744 | tf_op jit(solution)/shard_map/all_gather | solution.py:68
  27.5 84.8 %all-gather.7.cloned.1.call-done = bf16[4096,1152]{1,0:T(8,128)(2,1)} async-done(((bf16[64,1152]{1,0:T(8,128)(2,1)}), bf16[4096,1152]{1,0:T(8,128)(2,1)}) %all-gather.7.cloned.1.call-update) | async-done | bytes 9437200 | tf_op jit(solution)/shard_map/all_gather | solution.py:21
  112.3 4.0 %fusion.23 = f32[384,768]{1,0:T(8,128)S(1)} fusion(bf16[768,2048]{1,0:T(8,128)(2,1)} %all-gather.9.cloned.1.call-done, bf16[4096,1152]{1,0:T(8,128)(2,1)} %all-gather.7.cloned.1.call-done), kind=kOutput, calls=%fused_computation.29 | convolution fusion | flops 1207959552 | bytes 5898240 | tf_op jit(solution)/shard_map/dot_general | solution.py:48
  116.3 2.9 fusion.50
  119.2 1.8 fusion.96
  121.0 2.9 fusion.15
  123.9 2.9 fusion.47
  126.8 1.8 fusion.95
  128.6 51.8 %all-gather.11.cloned.1.call-done = bf16[4096,384]{1,0:T(8,128)(2,1)} async-done(((bf16[64,384]{1,0:T(8,128)(2,1)}), bf16[4096,384]{1,0:T(8,128)(2,1)}) %all-gather.11.cloned.1.call-update) | async-done | bytes 3145744 | tf_op jit(solution)/shard_map/all_gather | solution.py:21
  180.3 10.2 %fusion.21 = f32[768,2048]{1,0:T(8,128)} fusion(bf16[4096,384]{1,0:T(8,128)(2,1)} %all-gather.11.cloned.1.call-done, bf16[768,2048]{1,0:T(8,128)(2,1)} %all-gather.9.cloned.1.call-done, bf16[4096,1152]{1,0:T(8,128)(2,1)} %all-gather.7.cloned.1.call-done, f32[767,384]{0,1:T(8,128)} %get-tuple-element.14, f32[768,384]{0,1:T(8,128)S(1)} %fusion.50, ...), kind=kOutput, calls=%fused_computation.27 | convolution fusion | flops 2418573312 | bytes 16128000 | tf_op jit(solution)/shard_map/dot_general | solution.py:52
  190.6 11.4 %add_convert_fusion.1 = bf16[768,2048]{1,0:T(8,128)(2,1)} fusion(f32[768,2048]{1,0:T(8,128)} %fusion.21, bf16[4096,384]{1,0:T(8,128)(2,1)} %all-gather.11.cloned.1.call-done, bf16[768,2048]{1,0:T(8,128)(2,1)} %all-gather.9.cloned.1.call-done, bf16[4096,1152]{1,0:T(8,128)(2,1)} %all-gather.7.cloned.1.call-done, f32[767,384]{0,1:T(8,128)} %get-tuple-element.12, ...), kind=kOutput, calls=%fused_computation.3 | convolution fusion | flops 2421719040 | bytes 19273728 | tf_op jit(solution)/shard_map/dot_general | solution.py:52
  201.9 9.3 %all_to_all.10 = bf16[2,384,2048]{2,1,0:T(8,128)(2,1)S(1)} all-to-all(bf16[2,384,2048]{2,1,0:T(8,128)(2,1)} %bitcast.36), channel_id=1, replica_groups=mesh['rep'=2,'fs_0'=2,'fs_1'=4,'fs_2'=4,'tp'=2] {'tp'}, dimensions={0} | all-to-all | bytes 6291456 | tf_op jit(solution)/shard_map/all_to_all | solution.py:27
  211.2 0.7 convert_reduce_fusion.1
  211.9 0.7 copy-done.3
  212.6 0.5 fusion.70
  213.1 0.7 multiply_reduce_fusion.1
  213.8 1.8 multiply_convert_fusion.3
  215.7 0.0 all-gather.13.cloned.1.call-update
  215.7 0.0 all-gather.17.cloned.1.call-start
  215.8 1.6 fusion.86
  217.4 0.0 all-gather.17.cloned.1.call-update
  217.4 42.8 %all-gather.15.cloned.1.call-done = bf16[4096,1024]{1,0:T(8,128)(2,1)} async-done(((bf16[64,1024]{1,0:T(8,128)(2,1)}), bf16[4096,1024]{1,0:T(8,128)(2,1)}) %all-gather.15.cloned.1.call-update) | async-done | bytes 8388624 | tf_op jit(solution)/shard_map/all_gather | solution.py:21
  260.2 16.5 %all-gather.13.cloned.1.call-done = bf16[768,2048]{1,0:T(8,128)(2,1)} async-done(((bf16[384,2048]{1,0:T(8,128)(2,1)}), bf16[768,2048]{1,0:T(8,128)(2,1)}) %all-gather.13.cloned.1.call-update) | async-done | bytes 3145744 | tf_op jit(solution)/shard_map/all_gather | solution.py:88
  276.7 6.7 %multiply_convert_fusion.1 = bf16[768,1024]{1,0:T(8,128)(2,1)S(1)} fusion(bf16[768,2048]{1,0:T(8,128)(2,1)} %all-gather.13.cloned.1.call-done, bf16[4096,1024]{1,0:T(8,128)(2,1)} %all-gather.15.cloned.1.call-done), kind=kOutput, calls=%fused_computation.14 | convolution fusion | flops 3223584768 | bytes 8912896 | tf_op jit(solution)/shard_map/dot_general | solution.py:48
  283.4 4.6 %multiply_convert_fusion.2 = bf16[768,1024]{1,0:T(8,128)(2,1)} fusion(bf16[768,2048]{1,0:T(8,128)(2,1)S(1)} %copy-done.9, bf16[4096,1024]{1,0:T(8,128)(2,1)S(1)} %copy-done.7), kind=kOutput, calls=%fused_computation.15 | convolution fusion | flops 3223584768 | bytes 8912896 | tf_op jit(solution)/shard_map/dot_general | solution.py:48
  288.0 70.6 %all-gather.17.cloned.1.call-done = bf16[4096,1024]{1,0:T(8,128)(2,1)} async-done(((bf16[64,1024]{1,0:T(8,128)(2,1)}), bf16[4096,1024]{1,0:T(8,128)(2,1)}) %all-gather.17.cloned.1.call-update) | async-done | bytes 8388624 | tf_op jit(solution)/shard_map/all_gather | solution.py:21
  358.6 5.4 %fusion = f32[768,2048]{1,0:T(8,128)S(1)} fusion(bf16[768,1024]{1,0:T(8,128)(2,1)S(1)} %multiply_convert_fusion.1, bf16[4096,1024]{1,0:T(8,128)(2,1)} %all-gather.17.cloned.1.call-done), kind=kOutput, calls=%fused_computation.4 | convolution fusion | flops 3221225472 | bytes 12058624 | tf_op jit(solution)/shard_map/dot_general | solution.py:52
  364.1 3.7 add_convert_fusion
  367.8 6.8 %all_to_all.11 = bf16[2,384,2048]{2,1,0:T(8,128)(2,1)S(1)} all-to-all(bf16[2,384,2048]{2,1,0:T(8,128)(2,1)S(1)} %bitcast.37), channel_id=1, replica_groups=mesh['rep'=2,'fs_0'=2,'fs_1'=4,'fs_2'=4,'tp'=2] {'tp'}, dimensions={0} | all-to-all | bytes 6291456 | tf_op jit(solution)/shard_map/all_to_all | solution.py:27
  374.6 0.7 convert_reduce_fusion
  375.3 0.7 copy-done.2
  376.0 0.5 fusion.71
  376.5 0.7 multiply_reduce_fusion
  377.2 1.8 multiply_convert_fusion
  (26 shorter events, 0.1 us)
Async XLA Ops:
  6.5 5.0 %copy-start = (f32[64,2048]{1,0:T(8,128)S(1)}, f32[64,2048]{1,0:T(8,128)}, u32[]{:S(2)}) copy-start(f32[64,2048]{1,0:T(8,128)} %param.17) | copy-start | bytes 1572868
  6.5 20.9 %all-gather.9.cloned.1.call-start = ((), (), s32[]{:S(2)}) async-start(), calls=%async_computation.3 | async-start | bytes 4718592 | tf_op jit(solution)/shard_map/all_gather | solution.py:68
  7.3 105.0 %all-gather.7.cloned.1.call-start = ((), (), s32[]{:S(2)}) async-start(), calls=%async_computation.2 | async-start | bytes 9584640 | tf_op jit(solution)/shard_map/all_gather | solution.py:21
  9.9 170.5 %all-gather.11.cloned.1.call-start = ((), (), s32[]{:S(2)}) async-start(), calls=%async_computation.4 | async-start | bytes 3194880 | tf_op jit(solution)/shard_map/all_gather | solution.py:21
  11.5 248.7 %all-gather.15.cloned.1.call-start = ((), (), s32[]{:S(2)}) async-start(), calls=%async_computation.6 | async-start | bytes 8519680 | tf_op jit(solution)/shard_map/all_gather | solution.py:21
  12.2 264.5 %all-gather.13.cloned.1.call-start = ((), (), s32[]{:S(2)}) async-start(), calls=%async_computation.5 | async-start | bytes 4718592 | tf_op jit(solution)/shard_map/all_gather | solution.py:88
  112.3 4.0 %copy-start.4 = (bf16[768,2048]{1,0:T(8,128)(2,1)S(1)}, bf16[768,2048]{1,0:T(8,128)(2,1)}, u32[]{:S(2)}) copy-start(bf16[768,2048]{1,0:T(8,128)(2,1)} %all-gather.9.cloned.1.call-done) | copy-start | bytes 9437188
  211.2 1.4 copy-start.3
  213.1 0.7 copy-start.5
  215.7 142.9 %all-gather.17.cloned.1.call-start = ((), (), s32[]{:S(2)}) async-start(), calls=%async_computation.7 | async-start | bytes 8519680 | tf_op jit(solution)/shard_map/all_gather | solution.py:21
  276.7 6.7 %copy-start.7 = (bf16[4096,1024]{1,0:T(8,128)(2,1)S(1)}, bf16[4096,1024]{1,0:T(8,128)(2,1)}, u32[]{:S(2)}) copy-start(bf16[4096,1024]{1,0:T(8,128)(2,1)} %all-gather.15.cloned.1.call-done) | copy-start | bytes 25165828
  276.7 6.7 %copy-start.9 = (bf16[768,2048]{1,0:T(8,128)(2,1)S(1)}, bf16[768,2048]{1,0:T(8,128)(2,1)}, u32[]{:S(2)}) copy-start(bf16[768,2048]{1,0:T(8,128)(2,1)} %all-gather.13.cloned.1.call-done) | copy-start | bytes 9437188
  358.6 5.4 %copy-start.8 = (bf16[4096,1024]{1,0:T(8,128)(2,1)S(1)}, bf16[4096,1024]{1,0:T(8,128)(2,1)}, u32[]{:S(2)}) copy-start(bf16[4096,1024]{1,0:T(8,128)(2,1)} %all-gather.17.cloned.1.call-done) | copy-start | bytes 25165828
  358.6 5.4 %copy-start.10 = (bf16[768,1024]{1,0:T(8,128)(2,1)S(1)}, bf16[768,1024]{1,0:T(8,128)(2,1)}, u32[]{:S(2)}) copy-start(bf16[768,1024]{1,0:T(8,128)(2,1)} %multiply_convert_fusion.2) | copy-start | bytes 4718596
  374.6 1.4 copy-start.2
  376.5 0.7 copy-start.6
  377.2 1.9 copy-start.1
Sparse Core Ops, SparseCore 0:
  9.0 18.4 all-gather.8
  30.2 82.0 all-gather.6
  115.1 65.2 all-gather.10
  183.1 77.0 all-gather.14
  261.7 14.9 all-gather.12
  279.4 79.1 all-gather.16
where the time goes:
time: 386 us
  waiting for transfers between devices  282 us (73%)
  matrix products  54.6 us (14%)
  blocking collectives  16.1 us (4%)
  between operations  13.7 us (4%)
  local copies, waits for them, and re-layouts  11.4 us (3%)
  other arithmetic  8.22 us (2%)
    all_gather x4, waiting for transfers between devices, gathered_halves(): full = lax.all_gather(x, REP_FS, axis=0, tiled=True)  250 us
    dot_general x4, matrix products, dot_t(): lax.dot_general(a, b, (((1,), (1,)), ((), ())), preferred_element_type=jn...  30.7 us
    dot_general x6, matrix products, dot(): return jnp.dot(a, b, preferred_element_type=jnp.float32)  24 us
    all_gather x1, waiting for transfers between devices, local(): grouped_first = lax.all_gather(first, 'tp', axis=0, tiled=True)  16.5 us
    all_to_all x2, blocking collectives, sum_at_owner(): lax.all_to_all(tiles, axis, split_axis=0, concat_axis=0, tiled=True)  16.1 us
    all_gather x1, waiting for transfers between devices, local(): grouped = lax.all_gather(tokens, 'tp', axis=0, tiled=True)  14.3 us
  transfers between devices with their start and end apart: 6, of which 6 were waited for; matrix products, arithmetic and copies ran while one was open for 16% of the time, Pallas kernels for 0%

commit v1 on v0

--- a/solution.py
+++ b/solution.py
@@ -85,7 +85,9 @@
         mixing = mixing + dot_t(mixed, mixout_full[h])
     mixing = sum_at_owner(mixing.astype(bf), "tp")
     first = layer_norm(residual_scale * tokens.astype(jnp.float32) + mixing, norm_first).astype(bf)
-    grouped_first = lax.all_gather(first, "tp", axis=0, tiled=True)
+    grouped_first = jnp.concatenate(
+        lax.all_to_all(jnp.stack([first] * lax.axis_size("tp")), "tp", 0, 0), axis=0
+    )
     lowered = 0.0
     for h in range(2):
         raised = jax.nn.relu(dot(grouped_first, up_full[h]))

time: 386 us -> 368 us (0.953)
  waiting for transfers between devices: 282 us -> 255 us
  starting transfers between devices: 0.21 us -> 5.79 us
    all_gather x1 -> x0, waiting for transfers between devices: 16.5 us -> none  [local(): grouped_first = lax.all_gather(first, 'tp', axis=0, tiled=True)]
    all_gather x4, waiting for transfers between devices: 250 us -> 241 us  [gathered_halves(): full = lax.all_gather(x, REP_FS, axis=0, tiled=True)]
    all_to_all x0 -> x1, starting transfers between devices: none -> 5.63 us  [local(): lax.all_to_all(jnp.stack([first] * lax.axis_size('tp')), 'tp', 0, 0)]
  transfers between devices with their start and end apart: 6 -> 6, of which waited for: 6 -> 5; matrix products, arithmetic and copies ran while one was open for 16% -> 17% of each run, Pallas kernels for 0% -> 0%
where the time goes in v1:
time: 368 us
  waiting for transfers between devices  255 us (69%)
  matrix products  58.1 us (16%)
  blocking collectives  16 us (4%)
  between operations  13.3 us (4%)
  local copies, waits for them, and re-layouts  9.99 us (3%)
  other arithmetic  9.04 us (2%)
  starting transfers between devices  5.79 us (2%)
    all_gather x4, waiting for transfers between devices, gathered_halves(): full = lax.all_gather(x, REP_FS, axis=0, tiled=True)  241 us
    dot_general x4, matrix products, dot_t(): lax.dot_general(a, b, (((1,), (1,)), ((), ())), preferred_element_type=jn...  31.2 us
    dot_general x6, matrix products, dot(): return jnp.dot(a, b, preferred_element_type=jnp.float32)  26.9 us
    all_to_all x2, blocking collectives, sum_at_owner(): lax.all_to_all(tiles, axis, split_axis=0, concat_axis=0, tiled=True)  16 us
    all_gather x1, waiting for transfers between devices, local(): grouped = lax.all_gather(tokens, 'tp', axis=0, tiled=True)  13.5 us
  transfers between devices with their start and end apart: 6, of which 5 were waited for; matrix products, arithmetic and copies ran while one was open for 17% of the time, Pallas kernels for 0%

profile of v1, /device:TPU:1, one launch (start us, length us, event | category | flops | bytes accessed | tf_op | source)
XLA Modules:
  0.0 367.6 jit_solution(9069098653794527446)
XLA Ops:
  6.5 0.0 copy-start
  6.5 0.0 all-gather.8.cloned.1.call-start
  6.5 0.7 all-gather.8.cloned.1.call-update
  7.3 0.0 all-gather.6.cloned.1.call-start
  7.3 0.9 dynamic-slice_convert_fusion.5
  8.2 1.0 dynamic-slice_convert_fusion.3
  9.2 0.7 pad_maximum_fusion.1
  9.9 0.0 all-gather.6.cloned.1.call-update
  9.9 0.0 all-gather.10.cloned.1.call-start
  9.9 1.5 fusion.87
  11.4 0.0 all-gather.10.cloned.1.call-update
  11.5 0.0 all-gather.12.cloned.1.call-start
  11.5 0.7 dynamic-slice_convert_fusion.1
  12.2 0.0 all-gather.12.cloned.1.call-update
  12.2 0.0 all-gather.14.cloned.1.call-start
  12.3 1.6 fusion.86
  13.9 0.0 all-gather.14.cloned.1.call-update
  14.0 13.5 %all-gather.8.cloned.1.call-done = bf16[768,2048]{1,0:T(8,128)(2,1)} async-done(((bf16[384,2048]{1,0:T(8,128)(2,1)}), bf16[768,2048]{1,0:T(8,128)(2,1)}) %all-gather.8.cloned.1.call-update) | async-done | bytes 3145744 | tf_op jit(solution)/shard_map/all_gather | solution.py:68
  27.5 84.8 %all-gather.6.cloned.1.call-done = bf16[4096,1152]{1,0:T(8,128)(2,1)} async-done(((bf16[64,1152]{1,0:T(8,128)(2,1)}), bf16[4096,1152]{1,0:T(8,128)(2,1)}) %all-gather.6.cloned.1.call-update) | async-done | bytes 9437200 | tf_op jit(solution)/shard_map/all_gather | solution.py:21
  112.3 4.0 %fusion.23 = f32[384,768]{1,0:T(8,128)S(1)} fusion(bf16[768,2048]{1,0:T(8,128)(2,1)} %all-gather.8.cloned.1.call-done, bf16[4096,1152]{1,0:T(8,128)(2,1)} %all-gather.6.cloned.1.call-done), kind=kOutput, calls=%fused_computation.30 | convolution fusion | flops 1207959552 | bytes 5898240 | tf_op jit(solution)/shard_map/dot_general | solution.py:48
  116.3 2.9 fusion.50
  119.2 1.7 fusion.96
  120.9 2.9 fusion.15
  123.9 2.9 fusion.47
  126.8 1.8 fusion.95
  128.6 51.7 %all-gather.10.cloned.1.call-done = bf16[4096,384]{1,0:T(8,128)(2,1)} async-done(((bf16[64,384]{1,0:T(8,128)(2,1)}), bf16[4096,384]{1,0:T(8,128)(2,1)}) %all-gather.10.cloned.1.call-update) | async-done | bytes 3145744 | tf_op jit(solution)/shard_map/all_gather | solution.py:21
  180.3 10.3 %fusion.21 = f32[768,2048]{1,0:T(8,128)} fusion(bf16[4096,384]{1,0:T(8,128)(2,1)} %all-gather.10.cloned.1.call-done, bf16[768,2048]{1,0:T(8,128)(2,1)} %all-gather.8.cloned.1.call-done, bf16[4096,1152]{1,0:T(8,128)(2,1)} %all-gather.6.cloned.1.call-done, f32[767,384]{0,1:T(8,128)} %get-tuple-element.14, f32[768,384]{0,1:T(8,128)S(1)} %fusion.50, ...), kind=kOutput, calls=%fused_computation.28 | convolution fusion | flops 2418573312 | bytes 16128000 | tf_op jit(solution)/shard_map/dot_general | solution.py:52
  190.6 11.4 %add_convert_fusion.1 = bf16[768,2048]{1,0:T(8,128)(2,1)} fusion(f32[768,2048]{1,0:T(8,128)} %fusion.21, bf16[4096,384]{1,0:T(8,128)(2,1)} %all-gather.10.cloned.1.call-done, bf16[768,2048]{1,0:T(8,128)(2,1)} %all-gather.8.cloned.1.call-done, bf16[4096,1152]{1,0:T(8,128)(2,1)} %all-gather.6.cloned.1.call-done, f32[767,384]{0,1:T(8,128)} %get-tuple-element.12, ...), kind=kOutput, calls=%fused_computation.3 | convolution fusion | flops 2421719040 | bytes 19273728 | tf_op jit(solution)/shard_map/dot_general | solution.py:52
  202.0 9.3 %all_to_all.15 = bf16[2,384,2048]{2,1,0:T(8,128)(2,1)S(1)} all-to-all(bf16[2,384,2048]{2,1,0:T(8,128)(2,1)} %bitcast.39), channel_id=1, replica_groups=mesh['rep'=2,'fs_0'=2,'fs_1'=4,'fs_2'=4,'tp'=2] {'tp'}, dimensions={0} | all-to-all | bytes 6291456 | tf_op jit(solution)/shard_map/all_to_all | solution.py:27
  211.3 0.7 convert_reduce_fusion.1
  212.0 0.7 copy-done.2
  212.7 0.5 fusion.70
  213.2 0.7 multiply_reduce_fusion.1
  213.9 0.7 multiply_convert_fusion.3
  214.6 2.0 pad_maximum_fusion
  216.6 5.6 %all-to-all-start.1 = ((bf16[2,384,2048]{2,1,0:T(8,128)(2,1)}), bf16[2,384,2048]{2,1,0:T(8,128)(2,1)}, u32[]{:S(2)}, u32[]{:S(2)}) async-start(bf16[2,384,2048]{2,1,0:T(8,128)(2,1)} %pad_maximum_fusion), calls=%async_computation.1 | async-start | bytes 6291456 | tf_op jit(solution)/shard_map/all_to_all | solution.py:89
  222.2 38.0 %all-gather.12.cloned.1.call-done = bf16[4096,1024]{1,0:T(8,128)(2,1)} async-done(((bf16[64,1024]{1,0:T(8,128)(2,1)}), bf16[4096,1024]{1,0:T(8,128)(2,1)}) %all-gather.12.cloned.1.call-update) | async-done | bytes 8388624 | tf_op jit(solution)/shard_map/all_gather | solution.py:21
  260.2 0.0 all-to-all-done.1
  260.2 7.8 %multiply_convert_fusion.1 = bf16[768,1024]{1,0:T(8,128)(2,1)} fusion(bf16[768,2048]{1,0:T(8,128)(2,1)} %bitcast.7, bf16[4096,1024]{1,0:T(8,128)(2,1)} %all-gather.12.cloned.1.call-done), kind=kOutput, calls=%fused_computation.15 | convolution fusion | flops 3223584768 | bytes 8912896 | tf_op jit(solution)/shard_map/dot_general | solution.py:48
  268.0 6.4 %multiply_convert_fusion.2 = bf16[768,1024]{1,0:T(8,128)(2,1)} fusion(bf16[768,2048]{1,0:T(8,128)(2,1)} %bitcast.7, bf16[4096,1024]{1,0:T(8,128)(2,1)S(1)} %copy-done.7), kind=kOutput, calls=%fused_computation.16 | convolution fusion | flops 3223584768 | bytes 8912896 | tf_op jit(solution)/shard_map/dot_general | solution.py:48
  274.4 66.4 %all-gather.14.cloned.1.call-done = bf16[4096,1024]{1,0:T(8,128)(2,1)} async-done(((bf16[64,1024]{1,0:T(8,128)(2,1)}), bf16[4096,1024]{1,0:T(8,128)(2,1)}) %all-gather.14.cloned.1.call-update) | async-done | bytes 8388624 | tf_op jit(solution)/shard_map/all_gather | solution.py:21
  340.9 5.9 %fusion = f32[768,2048]{1,0:T(8,128)S(1)} fusion(bf16[768,1024]{1,0:T(8,128)(2,1)} %multiply_convert_fusion.1, bf16[4096,1024]{1,0:T(8,128)(2,1)} %all-gather.14.cloned.1.call-done), kind=kOutput, calls=%fused_computation.4 | convolution fusion | flops 3221225472 | bytes 12058624 | tf_op jit(solution)/shard_map/dot_general | solution.py:52
  346.8 3.7 %add_convert_fusion = bf16[768,2048]{1,0:T(8,128)(2,1)S(1)} fusion(f32[768,2048]{1,0:T(8,128)S(1)} %fusion, bf16[768,1024]{1,0:T(8,128)(2,1)S(1)} %copy-done.9, bf16[4096,1024]{1,0:T(8,128)(2,1)S(1)} %copy-done.8), kind=kOutput, calls=%fused_computation.1 | convolution fusion | flops 3224371200 | bytes 15204352 | tf_op jit(solution)/shard_map/dot_general | solution.py:52
  350.5 6.7 %all_to_all.16 = bf16[2,384,2048]{2,1,0:T(8,128)(2,1)S(1)} all-to-all(bf16[2,384,2048]{2,1,0:T(8,128)(2,1)S(1)} %bitcast.40), channel_id=1, replica_groups=mesh['rep'=2,'fs_0'=2,'fs_1'=4,'fs_2'=4,'tp'=2] {'tp'}, dimensions={0} | all-to-all | bytes 6291456 | tf_op jit(solution)/shard_map/all_to_all | solution.py:27
  357.2 0.7 convert_reduce_fusion
  358.0 0.5 fusion.71
  358.5 0.7 multiply_reduce_fusion
  359.2 1.8 multiply_convert_fusion
  (24 shorter events, 0.1 us)
Async XLA Ops:
  6.5 5.0 %copy-start = (f32[64,2048]{1,0:T(8,128)S(1)}, f32[64,2048]{1,0:T(8,128)}, u32[]{:S(2)}) copy-start(f32[64,2048]{1,0:T(8,128)} %param.17) | copy-start | bytes 1572868
  6.5 7.4 %copy-start.6 = (f32[3,768]{1,0:T(4,128)S(1)}, f32[3,768]{1,0:T(4,128)}, u32[]{:S(2)}) copy-start(f32[3,768]{1,0:T(4,128)} %param.14) | copy-start | bytes 27652
  6.5 20.9 %all-gather.8.cloned.1.call-start = ((), (), s32[]{:S(2)}) async-start(), calls=%async_computation.4 | async-start | bytes 4718592 | tf_op jit(solution)/shard_map/all_gather | solution.py:68
  7.3 105.0 %all-gather.6.cloned.1.call-start = ((), (), s32[]{:S(2)}) async-start(), calls=%async_computation.3 | async-start | bytes 9584640 | tf_op jit(solution)/shard_map/all_gather | solution.py:21
  9.9 170.5 %all-gather.10.cloned.1.call-start = ((), (), s32[]{:S(2)}) async-start(), calls=%async_computation.5 | async-start | bytes 3194880 | tf_op jit(solution)/shard_map/all_gather | solution.py:21
  11.5 248.7 %all-gather.12.cloned.1.call-start = ((), (), s32[]{:S(2)}) async-start(), calls=%async_computation.6 | async-start | bytes 8519680 | tf_op jit(solution)/shard_map/all_gather | solution.py:21
  12.2 328.7 %all-gather.14.cloned.1.call-start = ((), (), s32[]{:S(2)}) async-start(), calls=%async_computation.7 | async-start | bytes 8519680 | tf_op jit(solution)/shard_map/all_gather | solution.py:21
  112.3 4.0 %copy-start.3 = (bf16[768,2048]{1,0:T(8,128)(2,1)S(1)}, bf16[768,2048]{1,0:T(8,128)(2,1)}, u32[]{:S(2)}) copy-start(bf16[768,2048]{1,0:T(8,128)(2,1)} %all-gather.8.cloned.1.call-done) | copy-start | bytes 9437188
  211.2 1.4 copy-start.2
  213.1 0.7 copy-start.4
  216.6 43.7 %all-to-all-start.1 = ((bf16[2,384,2048]{2,1,0:T(8,128)(2,1)}), bf16[2,384,2048]{2,1,0:T(8,128)(2,1)}, u32[]{:S(2)}, u32[]{:S(2)}) async-start(bf16[2,384,2048]{2,1,0:T(8,128)(2,1)} %pad_maximum_fusion), calls=%async_computation.1 | async-start | bytes 6291456 | tf_op jit(solution)/shard_map/all_to_all | solution.py:89
  260.2 7.8 %copy-start.7 = (bf16[4096,1024]{1,0:T(8,128)(2,1)S(1)}, bf16[4096,1024]{1,0:T(8,128)(2,1)}, u32[]{:S(2)}) copy-start(bf16[4096,1024]{1,0:T(8,128)(2,1)} %all-gather.12.cloned.1.call-done) | copy-start | bytes 25165828
  340.9 5.9 %copy-start.8 = (bf16[4096,1024]{1,0:T(8,128)(2,1)S(1)}, bf16[4096,1024]{1,0:T(8,128)(2,1)}, u32[]{:S(2)}) copy-start(bf16[4096,1024]{1,0:T(8,128)(2,1)} %all-gather.14.cloned.1.call-done) | copy-start | bytes 25165828
  340.9 5.9 %copy-start.9 = (bf16[768,1024]{1,0:T(8,128)(2,1)S(1)}, bf16[768,1024]{1,0:T(8,128)(2,1)}, u32[]{:S(2)}) copy-start(bf16[768,1024]{1,0:T(8,128)(2,1)} %multiply_convert_fusion.2) | copy-start | bytes 4718596
  358.4 0.7 copy-start.5
  359.2 1.9 copy-start.1
Sparse Core Ops, SparseCore 0:
  9.0 18.4 all-gather.7
  30.2 82.0 all-gather.5
  115.1 65.2 all-gather.9
  183.1 77.0 all-gather.11
  262.9 77.9 all-gather.13
